TPU v7x, 32 devices: a whole 2x2x4 slice. The times are simulated.
32 devices in a mesh: fs: 8 (over z, y), tp: 4 (over x, core).
Axes of the slice: x: 2, y: 2, z: 4, core: 2. Of those that a mesh axis runs over, the one named last changes fastest.
Arguments:
- x_late: bfloat16 [6144, 2048], P(('fs', 'tp')), may hold values from -6 to 6
- x_early: bfloat16 [6144, 2048], P(('fs', 'tp')), may hold values from -6 to 6
- w_gate: bfloat16 [2048, 5632], P('fs', 'tp'), may hold values from -0.125 to 0.125
- w_value: bfloat16 [2048, 5632], P('fs', 'tp'), may hold values from -0.125 to 0.125
- conv_taps: float32 [3, 5632], P(None, 'tp'), may hold values from -3 to 3
- grad_hidden: bfloat16 [6144, 5632], P('fs', 'tp'), may hold values from -6 to 6
- sum_gate: float32 [2048, 5632], P('fs', 'tp'), may hold values from -6 to 6
- sum_value: float32 [2048, 5632], P('fs', 'tp'), may hold values from -6 to 6
- sum_taps: float32 [3, 5632], P(None, 'tp'), may hold values from -6 to 6
Outputs:
- hidden_late: bfloat16 [6144, 5632], P('fs', 'tp')
- grad_early: bfloat16 [6144, 2048], P(('fs', 'tp'))
- new_sum_gate: float32 [2048, 5632], P('fs', 'tp')
- new_sum_value: float32 [2048, 5632], P('fs', 'tp')
- new_sum_taps: float32 [3, 5632], P(None, 'tp')
All inputs are finite; a program needn't handle non-finite values.
Results may differ from a plain program's by a relative error of at most 0.015.
Values may be sent and summed in bfloat16 or wider, within the bound.
A program may use at most 128 MiB of HBM per device.

v0:
```python
import math

import jax
import jax.numpy as jnp
from jax import lax
from jax.sharding import PartitionSpec as P

root_half = 0.7071067811865476
density_norm = 0.3989422804014327


def causal_mix(gate_rows, taps):
    width = taps.shape[0]
    length = gate_rows.shape[0]
    padded = jnp.pad(gate_rows.astype(jnp.float32), ((width - 1, 0), (0, 0)))
    mixed_pre = jnp.zeros((length, gate_rows.shape[1]), jnp.float32)
    for j in range(width):
        mixed_pre = mixed_pre + padded[j : j + length] * taps[j]
    return (mixed_pre, padded)


def gelu_slope(mixed_pre):
    return (
        0.5 * (1.0 + lax.erf(mixed_pre * root_half))
        + mixed_pre * jnp.exp(-0.5 * mixed_pre * mixed_pre) * density_norm
    )


def back_mix(slope_rows, taps, padded):
    width = taps.shape[0]
    length = slope_rows.shape[0]
    grown = jnp.pad(slope_rows, ((0, width - 1), (0, 0)))
    d_gate = jnp.zeros(slope_rows.shape, jnp.float32)
    for j in range(width):
        d_gate = d_gate + grown[width - 1 - j : width - 1 - j + length] * taps[j]
    tap_terms = jnp.stack(
        [jnp.sum(slope_rows * padded[j : j + length], axis=0) for j in range(width)]
    )
    return (d_gate, tap_terms)


def shards(x_late, x_early, w_gate, w_value, conv_taps, grad_hidden, sum_gate, sum_value, sum_taps):
    columns = w_gate.shape[1]
    factor = 1.0 / math.sqrt(x_late.shape[0] * lax.axis_size("fs") * lax.axis_size("tp"))
    gate_full, value_full = (
        lax.all_gather(w_gate, "fs", axis=0, tiled=True),
        lax.all_gather(w_value, "fs", axis=0, tiled=True),
    )
    block_rows = lax.all_gather(x_late, "tp", axis=0, tiled=True)
    gate_part = jnp.dot(block_rows, gate_full, preferred_element_type=jnp.float32).astype(
        jnp.bfloat16
    )
    value_part = jnp.dot(block_rows, value_full, preferred_element_type=jnp.float32).astype(
        jnp.bfloat16
    )
    projected = jnp.concatenate([gate_part, value_part], axis=1)
    gate_rows = projected[:, :columns]
    value_rows = projected[:, columns:]
    mixed_pre, padded = causal_mix(gate_rows, conv_taps)
    hidden = (jax.nn.gelu(mixed_pre, approximate=False) * value_rows.astype(jnp.float32)).astype(
        jnp.bfloat16
    )
    gathered = lax.all_gather(x_early, "tp", axis=0, tiled=True)
    gate_rows = jnp.dot(gathered, gate_full, preferred_element_type=jnp.float32).astype(
        jnp.bfloat16
    )
    value_rows = jnp.dot(gathered, value_full, preferred_element_type=jnp.float32).astype(
        jnp.bfloat16
    )
    mixed_pre, padded = causal_mix(gate_rows, conv_taps)
    upstream = grad_hidden.astype(jnp.float32)
    slope_rows = upstream * value_rows.astype(jnp.float32) * gelu_slope(mixed_pre)
    d_gate_f, tap_terms = back_mix(slope_rows, conv_taps, padded)
    d_gate = d_gate_f.astype(jnp.bfloat16)
    d_value = (upstream * jax.nn.gelu(mixed_pre, approximate=False)).astype(jnp.bfloat16)
    contract = (((1,), (1,)), ((), ()))
    grad_early = lax.psum_scatter(
        (
            lax.dot_general(d_gate, gate_full, contract, preferred_element_type=jnp.float32)
            + lax.dot_general(d_value, value_full, contract, preferred_element_type=jnp.float32)
        ).astype(jnp.bfloat16),
        "tp",
        scatter_dimension=0,
        tiled=True,
    )
    both_grads = jnp.concatenate([d_gate, d_value], axis=1)
    product = lax.dot_general(
        gathered, both_grads, (((0,), (0,)), ((), ())), preferred_element_type=jnp.float32
    )
    totals = lax.psum_scatter(
        (factor * product).astype(jnp.bfloat16), "fs", scatter_dimension=0, tiled=True
    ).astype(jnp.float32)
    gate_total = totals[:, :columns]
    value_total = totals[:, columns:]
    tap_total = lax.psum(factor * tap_terms, "fs")
    return (
        hidden,
        grad_early,
        sum_gate + gate_total,
        sum_value + value_total,
        sum_taps + tap_total,
    )


def solution(mesh):
    placed = (
        P(("fs", "tp"), None),
        P(("fs", "tp"), None),
        P("fs", "tp"),
        P("fs", "tp"),
        P(None, "tp"),
        P("fs", "tp"),
        P("fs", "tp"),
        P("fs", "tp"),
        P(None, "tp"),
    )
    return jax.shard_map(
        shards,
        mesh=mesh,
        in_specs=placed,
        out_specs=(
            P("fs", "tp"),
            P(("fs", "tp"), None),
            P("fs", "tp"),
            P("fs", "tp"),
            P(None, "tp"),
        ),
        check_vma=False,
    )
```

profile of v0, /device:TPU:0, one launch (start us, length us, event | category | flops | bytes accessed | tf_op | source)
XLA Modules:
  0.0 500.2 jit_solution(172343307863899647)
XLA Ops:
  10.0 0.9 slice_reduce_fusion.2
  10.9 29.9 %all-gather.11.cloned.1.call-done = bf16[768,2048]{1,0:T(8,128)(2,1)} async-done(((bf16[192,2048]{1,0:T(8,128)(2,1)}), bf16[768,2048]{1,0:T(8,128)(2,1)}) %all-gather.11.cloned.1.call-update) | async-done | bytes 3145744 | tf_op jit(solution)/shard_map/all_gather | solution.py:63
  40.8 94.5 %all-gather.7.cloned.1.call-done = bf16[2048,1408]{1,0:T(8,128)(2,1)} async-done(((bf16[256,1408]{1,0:T(8,128)(2,1)}), bf16[2048,1408]{1,0:T(8,128)(2,1)}) %all-gather.7.cloned.1.call-update) | async-done | bytes 5767184 | tf_op jit(solution)/shard_map/all_gather | solution.py:46
  135.3 8.4 %fusion.30 = f32[768,1408]{1,0:T(8,128)S(1)} fusion(bf16[768,2048]{1,0:T(8,128)(2,1)} %all-gather.11.cloned.1.call-done, bf16[2048,1408]{1,0:T(8,128)(2,1)} %all-gather.7.cloned.1.call-done), kind=kOutput, calls=%fused_computation.62 | convolution fusion | flops 4431347712 | bytes 13238272 | tf_op jit(solution)/shard_map/dot_general | solution.py:64
  143.8 2.0 copy-done
  145.7 11.8 %fusion.2 = (bf16[768,1408]{1,0:T(8,128)(2,1)}, f32[768,1408]{1,0:T(8,128)}) fusion(bf16[768,1408]{1,0:T(8,128)(2,1)S(1)} %copy-done.2, f32[768,1408]{1,0:T(8,128)S(1)} %fusion.30, f32[1408]{0:T(1024)S(1)} %get-tuple-element.14, f32[1408]{0:T(1024)S(1)} %get-tuple-element.15, f32[1408]{0:T(1024)S(1)} %get-tuple-element.13), kind=kLoop, calls=%fused_computation.9 | loop fusion | flops 77856768 | bytes 12993024 | tf_op jit(solution)/shard_map/convert_element_type | solution.py:75
  157.6 70.5 %all-gather.9.cloned.1.call-done = bf16[2048,1408]{1,0:T(8,128)(2,1)} async-done(((bf16[256,1408]{1,0:T(8,128)(2,1)}), bf16[2048,1408]{1,0:T(8,128)(2,1)}) %all-gather.9.cloned.1.call-update) | async-done | bytes 5767184 | tf_op jit(solution)/shard_map/all_gather | solution.py:47
  228.0 9.8 %fusion.1 = f32[768,1408]{1,0:T(8,128)S(1)} fusion(bf16[768,1408]{1,0:T(8,128)(2,1)S(1)} %copy-done.2, f32[768,1408]{1,0:T(8,128)} %get-tuple-element.17, bf16[768,2048]{1,0:T(8,128)(2,1)} %all-gather.11.cloned.1.call-done, bf16[2048,1408]{1,0:T(8,128)(2,1)} %all-gather.9.cloned.1.call-done), kind=kOutput, calls=%fused_computation.8 | convolution fusion | flops 4443242496 | bytes 19726336 | tf_op jit(solution)/shard_map/dot_general | solution.py:67
  237.9 3.0 multiply_reduce_fusion.2
  240.9 1.3 copy-done.4
  242.3 12.1 %fusion = bf16[2048,2816]{0,1:T(8,128)(2,1)} fusion(bf16[768,2048]{1,0:T(8,128)(2,1)S(1)} %copy-done.7, bf16[768,1408]{1,0:T(8,128)(2,1)S(1)} %copy-done.3, bf16[768,1408]{1,0:T(8,128)(2,1)S(1)} %get-tuple-element.18), kind=kOutput, calls=%fused_computation.1 | convolution fusion | flops 8878555136 | bytes 19005440 | tf_op jit(solution)/shard_map/dot_general | solution.py:87
  254.5 7.8 %fusion.33 = f32[768,2048]{1,0:T(8,128)S(1)} fusion(bf16[768,1408]{1,0:T(8,128)(2,1)} %copy-done.4, bf16[2048,1408]{1,0:T(8,128)(2,1)} %all-gather.7.cloned.1.call-done), kind=kOutput, calls=%fused_computation.74 | convolution fusion | flops 4429185024 | bytes 14221312 | tf_op jit(solution)/shard_map/dot_general | solution.py:79
  262.3 9.2 %add_convert_fusion = bf16[768,2048]{1,0:T(8,128)(2,1)} fusion(f32[768,2048]{1,0:T(8,128)S(1)} %fusion.33, bf16[768,1408]{1,0:T(8,128)(2,1)S(1)} %copy-done.3, bf16[2048,1408]{1,0:T(8,128)(2,1)} %all-gather.9.cloned.1.call-done), kind=kOutput, calls=%fused_computation.5 | convolution fusion | flops 4432330752 | bytes 17367040 | tf_op jit(solution)/shard_map/dot_general | solution.py:80
  271.5 1.8 copy.14
  273.3 1.8 copy.15
  275.2 36.6 %psum.7 = f32[3,1408]{1,0:T(4,128)S(1)} all-reduce(f32[3,1408]{1,0:T(4,128)S(1)} %maximum_multiply_fusion), channel_id=1, replica_groups=mesh['fs'=8,'tp'=4] {'fs'}, use_global_device_ids=true, to_apply=%region_5.6 | all-reduce | flops 4224 | bytes 33792 | tf_op jit(solution)/shard_map/psum | solution.py:95
  312.4 9.0 %fusion.31 = f32[768,1408]{1,0:T(8,128)S(1)} fusion(bf16[768,2048]{1,0:T(8,128)(2,1)} %all-gather.5.cloned.1.call-done, bf16[2048,1408]{1,0:T(8,128)(2,1)} %all-gather.7.cloned.1.call-done), kind=kOutput, calls=%fused_computation.66 | convolution fusion | flops 4431347712 | bytes 13238272 | tf_op jit(solution)/shard_map/dot_general | solution.py:50
  321.4 19.9 %fusion.6 = bf16[768,1408]{1,0:T(8,128)(2,1)} fusion(f32[768,1408]{1,0:T(8,128)S(1)} %fusion.31, bf16[768,2048]{1,0:T(8,128)(2,1)S(1)} %copy-done.6, bf16[2048,1408]{1,0:T(8,128)(2,1)} %all-gather.9.cloned.1.call-done, f32[1408]{0:T(1024)S(1)} %get-tuple-element.14, f32[1408]{0:T(1024)S(1)} %get-tuple-element.15, f32[1408]{0:T(1024)S(1)} %get-tuple-element.13), kind=kOutput, calls=%fused_computation.13 | convolution fusion | flops 4508123136 | bytes 15417856 | tf_op jit(solution)/shard_map/dot_general | solution.py:53
  341.3 112.0 %reduce-scatter.5.cloned.1.call-done = bf16[256,2816]{0,1:T(8,128)(2,1)} async-done(((bf16[2048,2816]{0,1:T(8,128)(2,1)}), bf16[256,2816]{0,1:T(8,128)(2,1)}) %reduce-scatter.5.cloned.1.call-update) | async-done | bytes 1441808 | tf_op jit(solution)/shard_map/reduce_scatter | solution.py:90
  453.4 1.6 convert_element_type.68
  454.9 1.9 slice_add_fusion
  456.9 2.9 copy.16
  459.8 3.2 copy.17
  463.0 30.4 %reduce-scatter.3.cloned.1.call-done = bf16[192,2048]{1,0:T(8,128)(2,1)} async-done(((bf16[768,2048]{1,0:T(8,128)(2,1)}), bf16[192,2048]{1,0:T(8,128)(2,1)}) %reduce-scatter.3.cloned.1.call-update) | async-done | bytes 786448 | tf_op jit(solution)/shard_map/reduce_scatter | solution.py:77
  (32 shorter events, 3.5 us)
Async XLA Ops:
  7.2 33.6 %all-gather.11.cloned.1.call-start = ((), (), s32[]{:S(2)}) async-start(), calls=%async_computation.5 | async-start | bytes 3932160 | tf_op jit(solution)/shard_map/all_gather | solution.py:63
  7.9 127.4 %all-gather.7.cloned.1.call-start = ((), (), s32[]{:S(2)}) async-start(), calls=%async_computation.3 | async-start | bytes 6488064 | tf_op jit(solution)/shard_map/all_gather | solution.py:46
  8.6 219.4 %all-gather.9.cloned.1.call-start = ((), (), s32[]{:S(2)}) async-start(), calls=%async_computation.4 | async-start | bytes 6488064 | tf_op jit(solution)/shard_map/all_gather | solution.py:47
  9.4 303.0 %all-gather.5.cloned.1.call-start = ((), (), s32[]{:S(2)}) async-start(), calls=%async_computation.2 | async-start | bytes 3932160 | tf_op jit(solution)/shard_map/all_gather | solution.py:49
  10.0 443.4 %reduce-scatter.5.cloned.1.call-start = ((), (), s32[]{:S(2)}) async-start(), calls=%async_computation.7 | async-start | bytes 12976128 | tf_op jit(solution)/shard_map/reduce_scatter | solution.py:90
  10.9 134.8 %copy-start.2 = (bf16[768,1408]{1,0:T(8,128)(2,1)S(1)}, bf16[768,1408]{1,0:T(8,128)(2,1)}, u32[]{:S(2)}) copy-start(bf16[768,1408]{1,0:T(8,128)(2,1)} %param.14) | copy-start | bytes 6488068
  143.7 2.0 copy-start
  228.0 9.9 %copy-start.1 = (f32[768,1408]{1,0:T(8,128)S(1)}, f32[768,1408]{1,0:T(8,128)}, u32[]{:S(2)}) copy-start(f32[768,1408]{1,0:T(8,128)} %copy-done) | copy-start | bytes 12976132
  237.9 4.4 copy-start.3
  237.9 4.4 copy-start.7
  240.9 1.3 copy-start.4
  254.4 238.9 %reduce-scatter.3.cloned.1.call-start = ((), (), s32[]{:S(2)}) async-start(), calls=%async_computation.6 | async-start | bytes 3932160 | tf_op jit(solution)/shard_map/reduce_scatter | solution.py:77
  271.5 40.3 %copy-start.5 = (f32[3,1408]{1,0:T(4,128)S(1)}, f32[3,1408]{1,0:T(4,128)}, u32[]{:S(2)}) copy-start(f32[3,1408]{1,0:T(4,128)} %param.17) | copy-start | bytes 50692
  312.4 9.0 %copy-start.6 = (bf16[768,2048]{1,0:T(8,128)(2,1)S(1)}, bf16[768,2048]{1,0:T(8,128)(2,1)}, u32[]{:S(2)}) copy-start(bf16[768,2048]{1,0:T(8,128)(2,1)} %all-gather.5.cloned.1.call-done) | copy-start | bytes 9437188
Sparse Core Ops, SparseCore 0:
  9.5 31.2 all-gather.10
  43.0 92.3 all-gather.6
  137.5 90.4 all-gather.8
  229.4 26.6 all-gather.4
  259.6 193.6 reduce-scatter.4
  456.3 37.0 reduce-scatter.2
where the time goes:
time: 501 us; the launch traced here: 500 us
  waiting for transfers between devices  340 us (68%)
  matrix products  76.3 us (15%)
  blocking collectives  36.6 us (7%)
  other arithmetic  19 us (4%)
  between operations  14.3 us (3%)
  local copies, waits for them, and re-layouts  14 us (3%)
    reduce_scatter x1, waiting for transfers between devices, shards(): lax.psum_scatter((factor * product).astype(jnp.bfloat16), 'fs', scatter_d...  112 us
    all_gather x1, waiting for transfers between devices, shards(): lax.all_gather(w_gate, 'fs', axis=0, tiled=True)  94.5 us
    all_gather x1, waiting for transfers between devices, shards(): lax.all_gather(w_value, 'fs', axis=0, tiled=True)  70.5 us
    psum x1, blocking collectives, shards(): tap_total = lax.psum(factor * tap_terms, 'fs')  36.6 us
    reduce_scatter x1, waiting for transfers between devices, shards(): lax.psum_scatter((lax.dot_general(d_gate, gate_full, contract, preferred_...  30.4 us
    all_gather x1, waiting for transfers between devices, shards(): gathered = lax.all_gather(x_early, 'tp', axis=0, tiled=True)  29.9 us
    dot_general x1, matrix products, shards(): jnp.dot(block_rows, value_full, preferred_element_type=jnp.float32)  19.9 us
    unnamed x20, local copies, waits for them, and re-layouts  13.1 us
  transfers between devices with their start and end apart: 6, of which 5 were waited for; matrix products, arithmetic and copies ran while one was open for 21% of the time, Pallas kernels for 0%

commit v1 on v0

--- a/solution.py
+++ b/solution.py
@@ -1,8 +1,11 @@
 import math
+import functools
 
 import jax
 import jax.numpy as jnp
 from jax import lax
+from jax.experimental import pallas as pl
+from jax.experimental.pallas import tpu as pltpu
 from jax.sharding import PartitionSpec as P
 
 root_half = 0.7071067811865476
@@ -39,13 +42,351 @@
     return (d_gate, tap_terms)
 
 
+MESH = pl.DeviceIdType.MESH
+
+
+def greet(n, me):
+    barrier = pltpu.get_barrier_semaphore()
+    for away in range(1, n):
+        pl.semaphore_signal(
+            barrier, inc=1, device_id={"fs": lax.rem(me + away, n)}, device_id_type=MESH
+        )
+    pl.semaphore_wait(barrier, n - 1)
+
+
+def gather_kernel(n, *refs):
+    mine, full = refs[:2], refs[2:4]
+    up_out, up_in, down_out, down_in, y_out, y_in, cross_out, cross_in, own = refs[4:]
+    rows = mine[0].shape[0]
+    depth = n // 2
+    me = lax.axis_index("fs")
+    z, y = lax.div(me, 2), lax.rem(me, 2)
+    even = lax.rem(z, 2) == 0
+    mate = jnp.where(even, z + 1, z - 1)
+
+    def slot(p, zz, yy):
+        return full[p].at[pl.ds(pl.multiple_of((zz * 2 + yy) * rows, rows), rows)]
+
+    def link(p, source, zz, yy, out_sem, in_sem, to_z, to_y):
+        return pltpu.make_async_remote_copy(
+            src_ref=source,
+            dst_ref=slot(p, zz, yy),
+            send_sem=out_sem,
+            recv_sem=in_sem,
+            device_id={"fs": to_z * 2 + to_y},
+            device_id_type=MESH,
+        )
+
+    def up(p, k):
+        source = mine[p] if k == 0 else slot(p, z - k, y)
+        return link(p, source, z - k, y, up_out.at[p, k], up_in.at[p, k], z + 1, y)
+
+    def down(p, k):
+        source = mine[p] if k == 0 else slot(p, z + k, y)
+        return link(p, source, z + k, y, down_out.at[p, k], down_in.at[p, k], z - 1, y)
+
+    def over(p, j, zz):
+        source = mine[p] if j == 0 else slot(p, zz, y)
+        return link(p, source, zz, y, y_out.at[p, j], y_in.at[p, j], z, 1 - y)
+
+    def arrived(p, zz, yy, out_sem, in_sem):
+        return link(p, slot(p, zz, yy), zz, yy, out_sem, in_sem, z, 1 - y)
+
+    def cross():
+        return link(1, slot(1, z, 1 - y), z, 1 - y, cross_out, cross_in, mate, y)
+
+    greet(n, me)
+    for p in range(2):
+        pl.when(z + 1 < depth)(lambda p=p: up(p, 0).start())
+        pl.when(z > 0)(lambda p=p: down(p, 0).start())
+    for p in (1, 0):
+        over(p, 0, z).start()
+    local = [pltpu.make_async_copy(mine[p], slot(p, z, y), own.at[p]) for p in range(2)]
+    for copy in local:
+        copy.start()
+
+    def y_sent(p, k, upward):
+        if k == 0 and p == 1:
+            return even if upward else jnp.logical_not(even)
+        return None
+
+    for k in range(depth - 1):
+        for p in range(2):
+
+            @pl.when(z - 1 - k >= 0)
+            def _():
+                zz = z - 1 - k
+                arrived(p, zz, y, up_out.at[p, k], up_in.at[p, k]).wait_recv()
+                pl.when(z + 1 < depth)(lambda: up(p, k + 1).start())
+                wanted = y_sent(p, k, True)
+                send = lambda: over(p, 1 + 2 * k, zz).start()
+                send() if wanted is None else pl.when(wanted)(send)
+
+            @pl.when(z + 1 + k < depth)
+            def _():
+                zz = z + 1 + k
+                arrived(p, zz, y, down_out.at[p, k], down_in.at[p, k]).wait_recv()
+                pl.when(z > 0)(lambda: down(p, k + 1).start())
+                wanted = y_sent(p, k, False)
+                send = lambda: over(p, 2 + 2 * k, zz).start()
+                send() if wanted is None else pl.when(wanted)(send)
+
+        if k == 0:
+            arrived(1, z, 1 - y, y_out.at[1, 0], y_in.at[1, 0]).wait_recv()
+            cross().start()
+
+    arrived(0, z, 1 - y, y_out.at[0, 0], y_in.at[0, 0]).wait_recv()
+    for k in range(depth - 1):
+        for p in range(2):
+
+            @pl.when(z - 1 - k >= 0)
+            def _():
+                wanted = y_sent(p, k, True)
+                take = lambda: arrived(
+                    p, z - 1 - k, 1 - y, y_out.at[p, 1 + 2 * k], y_in.at[p, 1 + 2 * k]
+                ).wait_recv()
+                take() if wanted is None else pl.when(wanted)(take)
+
+            @pl.when(z + 1 + k < depth)
+            def _():
+                wanted = y_sent(p, k, False)
+                take = lambda: arrived(
+                    p, z + 1 + k, 1 - y, y_out.at[p, 2 + 2 * k], y_in.at[p, 2 + 2 * k]
+                ).wait_recv()
+                take() if wanted is None else pl.when(wanted)(take)
+
+    arrived(1, mate, 1 - y, cross_out, cross_in).wait_recv()
+    cross().wait_send()
+    for p in range(2):
+        over(p, 0, z).wait_send()
+        pl.when(z + 1 < depth)(lambda p=p: up(p, 0).wait_send())
+        pl.when(z > 0)(lambda p=p: down(p, 0).wait_send())
+        local[p].wait()
+        for k in range(depth - 1):
+
+            @pl.when(z - 1 - k >= 0)
+            def _():
+                pl.when(z + 1 < depth)(lambda: up(p, k + 1).wait_send())
+                wanted = y_sent(p, k, True)
+                end = lambda: over(p, 1 + 2 * k, z - 1 - k).wait_send()
+                end() if wanted is None else pl.when(wanted)(end)
+
+            @pl.when(z + 1 + k < depth)
+            def _():
+                pl.when(z > 0)(lambda: down(p, k + 1).wait_send())
+                wanted = y_sent(p, k, False)
+                end = lambda: over(p, 2 + 2 * k, z + 1 + k).wait_send()
+                end() if wanted is None else pl.when(wanted)(end)
+
+
+def gather_rows(w_gate, w_value):
+    n = lax.axis_size("fs")
+    depth = n // 2
+    rows, columns = w_gate.shape
+    sems = pltpu.SemaphoreType.DMA
+    whole = jax.ShapeDtypeStruct((n * rows, columns), w_gate.dtype)
+    hbm = pl.BlockSpec(memory_space=pl.ANY)
+    return pl.pallas_call(
+        functools.partial(gather_kernel, n),
+        out_shape=(whole, whole),
+        in_specs=[hbm, hbm],
+        out_specs=(hbm, hbm),
+        scratch_shapes=[
+            sems((2, depth)),
+            sems((2, depth)),
+            sems((2, depth)),
+            sems((2, depth)),
+            sems((2, 2 * depth)),
+            sems((2, 2 * depth)),
+            sems,
+            sems,
+            sems((2,)),
+        ],
+        compiler_params=pltpu.CompilerParams(collective_id=0, has_side_effects=True),
+        name="gather_rows",
+    )(w_gate, w_value)
+
+
+def scatter_kernel(n, *refs):
+    terms, taps, total, taps_total = refs[:2], refs[2], refs[3:5], refs[5]
+    y_got, up_got, down_got, taps_got = refs[6:8], refs[8:10], refs[10:12], refs[12]
+    y_out, y_in, z_out, up_in, down_in, taps_out, taps_in = refs[13:]
+    rows = total[0].shape[0]
+    depth = n // 2
+    step = math.gcd(rows, 32)
+    me = lax.axis_index("fs")
+    z, y = lax.div(me, 2), lax.rem(me, 2)
+
+    def start_of(zz, yy):
+        return pl.multiple_of((zz * 2 + yy) * rows, rows)
+
+    def over(p, zz):
+        return pltpu.make_async_remote_copy(
+            src_ref=terms[p].at[pl.ds(start_of(zz, 1 - y), rows)],
+            dst_ref=y_got[p].at[zz],
+            send_sem=y_out.at[p, zz],
+            recv_sem=y_in.at[p, zz],
+            device_id={"fs": z * 2 + 1 - y},
+            device_id_type=MESH,
+        )
+
+    def along(p, zz, away, upward):
+        got, sem = (up_got, up_in) if upward else (down_got, down_in)
+        return pltpu.make_async_remote_copy(
+            src_ref=y_got[p].at[zz],
+            dst_ref=got[p].at[away - 1],
+            send_sem=z_out.at[p, zz],
+            recv_sem=sem.at[p, away - 1],
+            device_id={"fs": (z + 1 if upward else z - 1) * 2 + y},
+            device_id_type=MESH,
+        )
+
+    def taps_copy(away):
+        return pltpu.make_async_remote_copy(
+            src_ref=taps,
+            dst_ref=taps_got.at[me],
+            send_sem=taps_out.at[away],
+            recv_sem=taps_in.at[me],
+            device_id={"fs": lax.rem(me + away, n)},
+            device_id_type=MESH,
+        )
+
+    def add(p, zz, others, into):
+        base = start_of(zz, y)
+
+        def body(i, _):
+            part = pl.ds(pl.multiple_of(i * step, step), step)
+            value = terms[p][
+                pl.ds(pl.multiple_of(base + i * step, step), step), :
+            ].astype(jnp.float32)
+            value = value + y_got[p][zz, part, :].astype(jnp.float32)
+            for ref, at in others:
+                value = value + ref[at, part, :].astype(jnp.float32)
+            if into is None:
+                y_got[p][zz, part, :] = value.astype(y_got[p].dtype)
+            else:
+                into[part, :] = value.astype(into.dtype)
+            return 0
+
+        lax.fori_loop(0, rows // step, body, 0)
+
+    greet(n, me)
+    for away in range(depth - 1, 0, -1):
+        for p in range(2):
+            pl.when(z + away < depth)(lambda: over(p, z + away).start())
+            pl.when(z - away >= 0)(lambda: over(p, z - away).start())
+    for p in range(2):
+        over(p, z).start()
+    for away in range(1, n):
+        taps_copy(away).start()
+
+    def pass_on(p, away, upward):
+        zz = z + away if upward else z - away
+        inside = zz < depth if upward else zz >= 0
+        has_more = z > 0 if upward else z + 1 < depth
+        got = up_got if upward else down_got
+
+        @pl.when(inside)
+        def _():
+            over(p, zz).wait_recv()
+
+            @pl.when(has_more)
+            def _():
+                if away < depth - 1:
+                    along(p, zz, away + 1, upward).wait_recv()
+                    add(p, zz, [(got[p], away)], None)
+
+            @pl.when(jnp.logical_not(has_more))
+            def _():
+                add(p, zz, [], None)
+
+            along(p, zz, away, upward).start()
+
+    for away in range(depth - 1, 0, -1):
+        for p in range(2):
+            pass_on(p, away, True)
+            pass_on(p, away, False)
+
+    taps_got[pl.ds(me, 1)] = taps[...][None]
+    for away in range(1, n):
+        source = lax.rem(me + away, n)
+        pltpu.make_async_remote_copy(
+            src_ref=taps,
+            dst_ref=taps_got.at[source],
+            send_sem=taps_out.at[away],
+            recv_sem=taps_in.at[source],
+            device_id={"fs": source},
+            device_id_type=MESH,
+        ).wait_recv()
+    sum_of = taps_got[0]
+    for i in range(1, n):
+        sum_of = sum_of + taps_got[i]
+    taps_total[...] = sum_of
+
+    for p in range(2):
+        over(p, z).wait_recv()
+        pl.when(z > 0)(lambda: along(p, z, 1, True).wait_recv())
+        pl.when(z + 1 < depth)(lambda: along(p, z, 1, False).wait_recv())
+        at_low, at_high = z == 0, z + 1 == depth
+        both = jnp.logical_not(jnp.logical_or(at_low, at_high))
+        pl.when(at_low)(lambda: add(p, z, [(down_got[p], 0)], total[p]))
+        pl.when(at_high)(lambda: add(p, z, [(up_got[p], 0)], total[p]))
+        pl.when(both)(lambda: add(p, z, [(up_got[p], 0), (down_got[p], 0)], total[p]))
+
+    for p in range(2):
+        over(p, z).wait_send()
+        for away in range(depth - 1, 0, -1):
+
+            @pl.when(z + away < depth)
+            def _():
+                over(p, z + away).wait_send()
+                along(p, z + away, away, True).wait_send()
+
+            @pl.when(z - away >= 0)
+            def _():
+                over(p, z - away).wait_send()
+                along(p, z - away, away, False).wait_send()
+
+    for away in range(1, n):
+        taps_copy(away).wait_send()
+
+
+def scatter_rows(gate_terms, value_terms, tap_terms):
+    n = lax.axis_size("fs")
+    depth = n // 2
+    rows, columns = gate_terms.shape[0] // n, gate_terms.shape[1]
+    sems = pltpu.SemaphoreType.DMA
+    vmem = pl.BlockSpec(memory_space=pltpu.VMEM)
+    total = jax.ShapeDtypeStruct((rows, columns), jnp.float32)
+    row_block = lambda count: pltpu.VMEM((count, rows, columns), gate_terms.dtype)
+    return pl.pallas_call(
+        functools.partial(scatter_kernel, n),
+        out_shape=(total, total, jax.ShapeDtypeStruct(tap_terms.shape, jnp.float32)),
+        in_specs=[vmem] * 3,
+        out_specs=(vmem,) * 3,
+        scratch_shapes=[row_block(depth)] * 2
+        + [row_block(depth - 1)] * 4
+        + [
+            pltpu.VMEM((n,) + tap_terms.shape, jnp.float32),
+            sems((2, depth)),
+            sems((2, depth)),
+            sems((2, depth)),
+            sems((2, depth)),
+            sems((2, depth)),
+            sems((n,)),
+            sems((n,)),
+        ],
+        compiler_params=pltpu.CompilerParams(
+            collective_id=1, has_side_effects=True, vmem_limit_bytes=60 * 1024 * 1024
+        ),
+        name="scatter_rows",
+    )(gate_terms, value_terms, tap_terms)
+
+
 def shards(x_late, x_early, w_gate, w_value, conv_taps, grad_hidden, sum_gate, sum_value, sum_taps):
     columns = w_gate.shape[1]
     factor = 1.0 / math.sqrt(x_late.shape[0] * lax.axis_size("fs") * lax.axis_size("tp"))
-    gate_full, value_full = (
-        lax.all_gather(w_gate, "fs", axis=0, tiled=True),
-        lax.all_gather(w_value, "fs", axis=0, tiled=True),
-    )
+    gate_full, value_full = gather_rows(w_gate, w_value)
     block_rows = lax.all_gather(x_late, "tp", axis=0, tiled=True)
     gate_part = jnp.dot(block_rows, gate_full, preferred_element_type=jnp.float32).astype(
         jnp.bfloat16
@@ -83,16 +424,16 @@
         scatter_dimension=0,
         tiled=True,
     )
-    both_grads = jnp.concatenate([d_gate, d_value], axis=1)
-    product = lax.dot_general(
-        gathered, both_grads, (((0,), (0,)), ((), ())), preferred_element_type=jnp.float32
-    )
-    totals = lax.psum_scatter(
-        (factor * product).astype(jnp.bfloat16), "fs", scatter_dimension=0, tiled=True
-    ).astype(jnp.float32)
-    gate_total = totals[:, :columns]
-    value_total = totals[:, columns:]
-    tap_total = lax.psum(factor * tap_terms, "fs")
+    outer = (((0,), (0,)), ((), ()))
+    gate_terms = lax.dot_general(gathered, d_gate, outer, preferred_element_type=jnp.float32)
+    value_terms = lax.dot_general(gathered, d_value, outer, preferred_element_type=jnp.float32)
+    taps_padded = jnp.pad(factor * tap_terms, ((0, -tap_terms.shape[0] % 8), (0, 0)))
+    gate_total, value_total, tap_total = scatter_rows(
+        (factor * gate_terms).astype(jnp.bfloat16),
+        (factor * value_terms).astype(jnp.bfloat16),
+        taps_padded,
+    )
+    tap_total = tap_total[: tap_terms.shape[0]]
     return (
         hidden,
         grad_early,

time: 501 us -> 379 us (0.76)
  waiting for transfers between devices: 340 us -> 1.42 us
  Pallas kernels: 0 us -> 269 us
  blocking collectives: 36.6 us -> 0 us
  local copies, waits for them, and re-layouts: 14 us -> 1.59 us
    pallas_call x0 -> x2, Pallas kernels: none -> 269 us  [the longest x1 137 us: scatter_rows(): pl.pallas_call(functools.partial(scatter_kernel, n), out_shape=(total, to...]
    all_gather x2 -> x0, waiting for transfers between devices: 165 us -> none  [the longest x1 94.5 us: shards(): lax.all_gather(w_gate, 'fs', axis=0, tiled=True)]
    reduce_scatter x1 -> x0, waiting for transfers between devices: 112 us -> none  [shards(): lax.psum_scatter((factor * product).astype(jnp.bfloat16), 'fs', scatter_d...]
    psum x1 -> x0, blocking collectives: 36.6 us -> none  [shards(): tap_total = lax.psum(factor * tap_terms, 'fs')]
    reduce_scatter x1, waiting for transfers between devices: 30.4 us -> 0.01 us  [shards(): lax.psum_scatter((lax.dot_general(d_gate, gate_full, contract, preferred_...]
    all_gather x1, waiting for transfers between devices: 29.9 us -> 0.02 us  [shards(): gathered = lax.all_gather(x_early, 'tp', axis=0, tiled=True)]
    unnamed x20 -> x22, local copies, waits for them, and re-layouts: 13.1 us -> 0.05 us
    dot_general x1 -> x2, matrix products: 12.1 us -> 16.2 us  [the longest x1 9.13 us: shards(): lax.dot_general(gathered, d_gate, outer, preferred_element_type=jnp.float32)]
  transfers between devices with their start and end apart: 6 -> 3, of which waited for: 5 -> 0; matrix products, arithmetic and copies ran while one was open for 21% -> 25% of each run, Pallas kernels for 0% -> 71%
where the time goes in v1:
time: 379 us
  Pallas kernels  269 us (71%)
  matrix products  74.3 us (20%)
  other arithmetic  18.6 us (5%)
  between operations  14 us (4%)
    pallas_call x1, Pallas kernels, scatter_rows(): pl.pallas_call(functools.partial(scatter_kernel, n), out_shape=(total, to...  137 us
    pallas_call x1, Pallas kernels, gather_rows(): pl.pallas_call(functools.partial(gather_kernel, n), out_shape=(whole, who...  132 us
    dot_general x1, matrix products, shards(): jnp.dot(block_rows, value_full, preferred_element_type=jnp.float32)  19.9 us
    convert_element_type x1, other arithmetic, shards(): (upstream * jax.nn.gelu(mixed_pre, approximate=False)).astype(jnp.bfloat16)  10.9 us
    dot_general x1, matrix products, shards(): lax.dot_general(gathered, d_gate, outer, preferred_element_type=jnp.float32)  9.13 us
    dot_general x1, matrix products, shards(): jnp.dot(block_rows, gate_full, preferred_element_type=jnp.float32)  8.98 us
    dot_general x1, matrix products, shards(): jnp.dot(gathered, gate_full, preferred_element_type=jnp.float32)  8.6 us
    dot_general x1, matrix products, shards(): lax.dot_general(d_gate, gate_full, contract, preferred_element_type=jnp.f...  7.85 us
  transfers between devices with their start and end apart: 3, of which 0 were waited for; matrix products, arithmetic and copies ran while one was open for 25% of the time, Pallas kernels for 71%

profile of v1, /device:TPU:0, one launch (start us, length us, event | category | flops | bytes accessed | tf_op | source)
XLA Modules:
  0.0 379.2 jit_solution(1954915939859520063)
XLA Ops:
  7.2 0.0 all-gather.5.cloned.1.call-start
  7.2 0.7 all-gather.5.cloned.1.call-update
  7.9 0.0 all-gather.3.cloned.1.call-start
  7.9 0.7 all-gather.3.cloned.1.call-update
  8.6 0.0 reduce-scatter.2.cloned.1.call-start
  8.7 0.9 slice_reduce_fusion.2
  9.6 132.3 %gather_rows.1 = (bf16[2048,1408]{1,0:T(8,128)(2,1)}, bf16[2048,1408]{1,0:T(8,128)(2,1)}) custom-call(bf16[256,1408]{1,0:T(8,128)(2,1)} %refs_0_.1, bf16[256,1408]{1,0:T(8,128)(2,1)} %refs_1_.1), custom_call_target="tpu_custom_call" | custom-call | tf_op jit(solution)/shard_map/gather_rows/pallas_call | solution.py:189
  141.9 0.0 all-gather.5.cloned.1.call-done
  142.0 8.6 %convert_bitcast_fusion = f32[768,1408]{1,0:T(8,128)S(1)} fusion(bf16[768,2048]{1,0:T(8,128)(2,1)} %all-gather.5.cloned.1.call-done, bf16[2048,1408]{1,0:T(8,128)(2,1)} %get-tuple-element.10), kind=kOutput, calls=%fused_computation.22 | convolution fusion | flops 4431347712 | bytes 13238272 | tf_op jit(solution)/shard_map/dot_general | solution.py:405
  150.6 10.9 %fusion.3 = (bf16[768,1408]{1,0:T(8,128)(2,1)S(1)}, f32[768,1408]{1,0:T(8,128)S(1)}) fusion(bf16[768,1408]{1,0:T(8,128)(2,1)S(1)} %copy-done, f32[768,1408]{1,0:T(8,128)S(1)} %convert_bitcast_fusion, f32[1408]{0:T(1024)S(1)} %get-tuple-element.19, f32[1408]{0:T(1024)S(1)} %get-tuple-element.20, f32[1408]{0:T(1024)S(1)} %get-tuple-element.18), kind=kLoop, calls=%fused_computation.11 | loop fusion | flops 77856768 | bytes 12993024 | tf_op jit(solution)/shard_map/convert_element_type | solution.py:416
  161.5 6.1 %fusion.2 = f32[768,1408]{1,0:T(8,128)S(1)} fusion(bf16[768,1408]{1,0:T(8,128)(2,1)S(1)} %copy-done, f32[768,1408]{1,0:T(8,128)S(1)} %get-tuple-element.22, bf16[768,2048]{1,0:T(8,128)(2,1)S(1)} %copy-done.9, bf16[2048,1408]{1,0:T(8,128)(2,1)S(1)} %copy-done.7), kind=kOutput, calls=%fused_computation.10 | convolution fusion | flops 4443242496 | bytes 19726336 | tf_op jit(solution)/shard_map/dot_general | solution.py:408
  167.6 2.9 multiply_reduce_fusion.2
  170.6 7.9 %fusion.28 = f32[768,2048]{1,0:T(8,128)S(1)} fusion(bf16[768,1408]{1,0:T(8,128)(2,1)S(1)} %get-tuple-element.23, bf16[2048,1408]{1,0:T(8,128)(2,1)} %get-tuple-element.10), kind=kOutput, calls=%fused_computation.71 | convolution fusion | flops 4429185024 | bytes 14221312 | tf_op jit(solution)/shard_map/dot_general | solution.py:420
  178.5 6.7 %add_convert_fusion = bf16[768,2048]{1,0:T(8,128)(2,1)} fusion(f32[768,2048]{1,0:T(8,128)S(1)} %fusion.28, bf16[768,1408]{1,0:T(8,128)(2,1)S(1)} %get-tuple-element.21, bf16[2048,1408]{1,0:T(8,128)(2,1)S(1)} %copy-done.7), kind=kOutput, calls=%fused_computation.7 | convolution fusion | flops 4432330752 | bytes 17367040 | tf_op jit(solution)/shard_map/dot_general | solution.py:421
  185.2 0.0 reduce-scatter.2.cloned.1.call-update
  185.2 9.1 %fusion.refs_0_ = bf16[2048,1408]{1,0:T(8,128)(2,1)} fusion(bf16[768,1408]{1,0:T(8,128)(2,1)} %copy-done.1, bf16[768,2048]{1,0:T(8,128)(2,1)} %all-gather.5.cloned.1.call-done), kind=kOutput, calls=%fused_computation.2 | convolution fusion | flops 4434952192 | bytes 11075584 | tf_op jit(solution)/shard_map/dot_general | solution.py:428
  194.4 0.6 pad.18.refs_2_
  195.0 7.0 %fusion.1.refs_1_ = bf16[2048,1408]{1,0:T(8,128)(2,1)} fusion(bf16[768,1408]{1,0:T(8,128)(2,1)S(1)} %get-tuple-element.21, bf16[768,2048]{1,0:T(8,128)(2,1)S(1)} %copy-done.10), kind=kOutput, calls=%fused_computation.3 | convolution fusion | flops 4434952192 | bytes 11075584 | tf_op jit(solution)/shard_map/dot_general | solution.py:429
  202.0 136.9 %scatter_rows.1 = (f32[256,1408]{1,0:T(8,128)}, f32[256,1408]{1,0:T(8,128)}, f32[8,1408]{1,0:T(8,128)}) custom-call(bf16[2048,1408]{1,0:T(8,128)(2,1)} %fusion.refs_0_, bf16[2048,1408]{1,0:T(8,128)(2,1)} %fusion.1.refs_1_, f32[8,1408]{1,0:T(8,128)} %pad.18.refs_2_), custom_call_target="tpu_custom_call" | custom-call | tf_op jit(solution)/shard_map/scatter_rows/pallas_call | solution.py:362
  339.0 2.9 add.55
  341.8 1.2 add.56
  343.1 0.6 slice_add_fusion
  343.7 9.0 %convert_bitcast_fusion.1 = f32[768,1408]{1,0:T(8,128)S(1)} fusion(bf16[768,2048]{1,0:T(8,128)(2,1)} %all-gather.3.cloned.1.call-done, bf16[2048,1408]{1,0:T(8,128)(2,1)} %get-tuple-element.10), kind=kOutput, calls=%fused_computation.23 | convolution fusion | flops 4431347712 | bytes 13238272 | tf_op jit(solution)/shard_map/dot_general | solution.py:391
  352.7 19.9 %fusion.7 = bf16[768,1408]{1,0:T(8,128)(2,1)} fusion(f32[768,1408]{1,0:T(8,128)S(1)} %convert_bitcast_fusion.1, bf16[768,2048]{1,0:T(8,128)(2,1)S(1)} %copy-done.8, bf16[2048,1408]{1,0:T(8,128)(2,1)} %get-tuple-element.11, f32[1408]{0:T(1024)S(1)} %get-tuple-element.19, f32[1408]{0:T(1024)S(1)} %get-tuple-element.20, f32[1408]{0:T(1024)S(1)} %get-tuple-element.18), kind=kOutput, calls=%fused_computation.15 | convolution fusion | flops 4508123136 | bytes 15417856 | tf_op jit(solution)/shard_map/dot_general | solution.py:394
  (28 shorter events, 0.1 us)
Async XLA Ops:
  7.2 134.8 %all-gather.5.cloned.1.call-start = ((), (), s32[]{:S(2)}) async-start(), calls=%async_computation.2 | async-start | bytes 3932160 | tf_op jit(solution)/shard_map/all_gather | solution.py:404
  7.9 335.8 %all-gather.3.cloned.1.call-start = ((), (), s32[]{:S(2)}) async-start(), calls=%async_computation.1 | async-start | bytes 3932160 | tf_op jit(solution)/shard_map/all_gather | solution.py:390
  8.6 364.0 %reduce-scatter.2.cloned.1.call-start = ((), (), s32[]{:S(2)}) async-start(), calls=%async_computation.3 | async-start | bytes 3932160 | tf_op jit(solution)/shard_map/reduce_scatter | solution.py:418
  141.9 8.6 %copy-start = (bf16[768,1408]{1,0:T(8,128)(2,1)S(1)}, bf16[768,1408]{1,0:T(8,128)(2,1)}, u32[]{:S(2)}) copy-start(bf16[768,1408]{1,0:T(8,128)(2,1)} %param.14) | copy-start | bytes 6488068
  150.6 10.9 %copy-start.7 = (bf16[2048,1408]{1,0:T(8,128)(2,1)S(1)}, bf16[2048,1408]{1,0:T(8,128)(2,1)}, u32[]{:S(2)}) copy-start(bf16[2048,1408]{1,0:T(8,128)(2,1)} %get-tuple-element.11) | copy-start | bytes 17301508
  150.6 10.9 %copy-start.9 = (bf16[768,2048]{1,0:T(8,128)(2,1)S(1)}, bf16[768,2048]{1,0:T(8,128)(2,1)}, u32[]{:S(2)}) copy-start(bf16[768,2048]{1,0:T(8,128)(2,1)} %all-gather.5.cloned.1.call-done) | copy-start | bytes 9437188
  170.6 7.9 %copy-start.1 = (bf16[768,1408]{1,0:T(8,128)(2,1)}, bf16[768,1408]{1,0:T(8,128)(2,1)S(1)}, u32[]{:S(2)}) copy-start(bf16[768,1408]{1,0:T(8,128)(2,1)S(1)} %get-tuple-element.23) | copy-start | bytes 6488068
  185.2 9.8 %copy-start.10 = (bf16[768,2048]{1,0:T(8,128)(2,1)S(1)}, bf16[768,2048]{1,0:T(8,128)(2,1)}, u32[]{:S(2)}) copy-start(bf16[768,2048]{1,0:T(8,128)(2,1)} %all-gather.5.cloned.1.call-done) | copy-start | bytes 9437188
  202.0 136.9 %copy-start.2 = (f32[256,1408]{1,0:T(8,128)S(1)}, f32[256,1408]{1,0:T(8,128)}, u32[]{:S(2)}) copy-start(f32[256,1408]{1,0:T(8,128)} %param.15) | copy-start | bytes 4325380
  338.9 2.9 copy-start.3
  338.9 2.9 copy-start.4
  338.9 4.2 %copy-start.5 = (f32[3,1408]{1,0:T(4,128)S(1)}, f32[3,1408]{1,0:T(4,128)}, u32[]{:S(2)}) copy-start(f32[3,1408]{1,0:T(4,128)} %param.17) | copy-start | bytes 50692
  338.9 4.1 %copy-start.6 = (f32[8,1408]{1,0:T(8,128)S(1)}, f32[8,1408]{1,0:T(8,128)}, u32[]{:S(2)}) copy-start(f32[8,1408]{1,0:T(8,128)} %get-tuple-element.14) | copy-start | bytes 135172
  343.7 9.0 %copy-start.8 = (bf16[768,2048]{1,0:T(8,128)(2,1)S(1)}, bf16[768,2048]{1,0:T(8,128)(2,1)}, u32[]{:S(2)}) copy-start(bf16[768,2048]{1,0:T(8,128)(2,1)} %all-gather.3.cloned.1.call-done) | copy-start | bytes 9437188
Sparse Core Ops, SparseCore 0:
  9.5 31.2 all-gather.4
  42.4 28.4 all-gather.2
  185.3 36.8 reduce-scatter.1

commit v2 on v1

--- a/solution.py
+++ b/solution.py
@@ -208,21 +208,70 @@
 
 
 def scatter_kernel(n, *refs):
-    terms, taps, total, taps_total = refs[:2], refs[2], refs[3:5], refs[5]
-    y_got, up_got, down_got, taps_got = refs[6:8], refs[8:10], refs[10:12], refs[12]
-    y_out, y_in, z_out, up_in, down_in, taps_out, taps_in = refs[13:]
+    terms, taps, rows_late, weights, conv = refs[:2], refs[2], refs[3], refs[4:6], refs[6]
+    total, taps_total, hidden = refs[7:9], refs[9], refs[10]
+    y_got, up_got, down_got, taps_got = refs[11:13], refs[13:15], refs[15:17], refs[17]
+    cross_got, strip = refs[18], refs[19]
+    y_out, y_in, z_out, up_in, down_in, taps_out, taps_in = refs[20:27]
+    cross_out, cross_in, strip_in = refs[27:]
     rows = total[0].shape[0]
     depth = n // 2
     step = math.gcd(rows, 32)
     me = lax.axis_index("fs")
     z, y = lax.div(me, 2), lax.rem(me, 2)
+    even = lax.rem(z, 2) == 0
+    odd = jnp.logical_not(even)
+    mate = jnp.where(even, z + 1, z - 1)
+    lane = 128
+    strips = hidden.shape[1] // lane
+
+    def fetch(b):
+        at = pl.ds(pl.multiple_of(b * lane, lane), lane)
+        slot = lax.rem(b, 2)
+        return [
+            pltpu.make_async_copy(
+                weights[i].at[:, at],
+                strip.at[slot, :, pl.ds(i * lane, lane)],
+                strip_in.at[slot, i],
+            )
+            for i in range(2)
+        ]
+
+    def late(first, last):
+        def body(b, _):
+            for copy in fetch(b):
+                copy.wait()
+
+            @pl.when(b + 1 < strips)
+            def _():
+                for copy in fetch(b + 1):
+                    copy.start()
+
+            at = pl.ds(pl.multiple_of(b * lane, lane), lane)
+            both = jnp.dot(
+                rows_late[...], strip[lax.rem(b, 2)], preferred_element_type=jnp.float32
+            )
+            both = both.astype(jnp.bfloat16).astype(jnp.float32)
+            gate = both[:, :lane]
+            width = conv.shape[0]
+            position = lax.broadcasted_iota(jnp.int32, gate.shape, 0)
+            pre = gate * conv[pl.ds(width - 1, 1), at]
+            for j in range(width - 1):
+                lag = width - 1 - j
+                moved = jnp.where(position >= lag, pltpu.roll(gate, lag, 0), 0.0)
+                pre = pre + moved * conv[pl.ds(j, 1), at]
+            active = 0.5 * pre * (1.0 + lax.erf(pre * root_half))
+            hidden[:, at] = (active * both[:, lane:]).astype(hidden.dtype)
+            return 0
+
+        lax.fori_loop(first, last, body, 0)
 
     def start_of(zz, yy):
         return pl.multiple_of((zz * 2 + yy) * rows, rows)
 
-    def over(p, zz):
+    def over(p, zz, source=None):
         return pltpu.make_async_remote_copy(
-            src_ref=terms[p].at[pl.ds(start_of(zz, 1 - y), rows)],
+            src_ref=terms[p].at[pl.ds(start_of(zz, 1 - y), rows)] if source is None else source,
             dst_ref=y_got[p].at[zz],
             send_sem=y_out.at[p, zz],
             recv_sem=y_in.at[p, zz],
@@ -241,6 +290,33 @@
             device_id_type=MESH,
         )
 
+    def cross():
+        return pltpu.make_async_remote_copy(
+            src_ref=terms[1].at[pl.ds(start_of(mate, 1 - y), rows)],
+            dst_ref=cross_got,
+            send_sem=cross_out,
+            recv_sem=cross_in,
+            device_id={"fs": mate * 2 + y},
+            device_id_type=MESH,
+        )
+
+    def add_cross():
+        base = start_of(z, 1 - y)
+
+        def body(i, _):
+            part = pl.ds(pl.multiple_of(i * step, step), step)
+            value = terms[1][pl.ds(pl.multiple_of(base + i * step, step), step), :]
+            value = value.astype(jnp.float32) + cross_got[part, :].astype(jnp.float32)
+            cross_got[part, :] = value.astype(cross_got.dtype)
+            return 0
+
+        lax.fori_loop(0, rows // step, body, 0)
+
+    def over_y(p, away, upward):
+        if p == 1 and away == 1:
+            return odd if upward else even
+        return True
+
     def taps_copy(away):
         return pltpu.make_async_remote_copy(
             src_ref=taps,
@@ -251,7 +327,7 @@
             device_id_type=MESH,
         )
 
-    def add(p, zz, others, into):
+    def add(p, zz, others, into, from_y=True):
         base = start_of(zz, y)
 
         def body(i, _):
@@ -259,7 +335,8 @@
             value = terms[p][
                 pl.ds(pl.multiple_of(base + i * step, step), step), :
             ].astype(jnp.float32)
-            value = value + y_got[p][zz, part, :].astype(jnp.float32)
+            if from_y:
+                value = value + y_got[p][zz, part, :].astype(jnp.float32)
             for ref, at in others:
                 value = value + ref[at, part, :].astype(jnp.float32)
             if into is None:
@@ -270,13 +347,20 @@
 
         lax.fori_loop(0, rows // step, body, 0)
 
+    for copy in fetch(0):
+        copy.start()
     greet(n, me)
+    cross().start()
     for away in range(depth - 1, 0, -1):
         for p in range(2):
-            pl.when(z + away < depth)(lambda: over(p, z + away).start())
-            pl.when(z - away >= 0)(lambda: over(p, z - away).start())
-    for p in range(2):
-        over(p, z).start()
+            up_too, down_too = over_y(p, away, True), over_y(p, away, False)
+            pl.when(jnp.logical_and(z + away < depth, up_too))(
+                lambda: over(p, z + away).start()
+            )
+            pl.when(jnp.logical_and(z - away >= 0, down_too))(
+                lambda: over(p, z - away).start()
+            )
+    over(0, z).start()
     for away in range(1, n):
         taps_copy(away).start()
 
@@ -285,27 +369,47 @@
         inside = zz < depth if upward else zz >= 0
         has_more = z > 0 if upward else z + 1 < depth
         got = up_got if upward else down_got
+        kinds = [(True, True)]
+        if p == 1 and away == 1:
+            kinds = [(True, odd if upward else even), (False, even if upward else odd)]
 
         @pl.when(inside)
         def _():
-            over(p, zz).wait_recv()
-
-            @pl.when(has_more)
-            def _():
-                if away < depth - 1:
-                    along(p, zz, away + 1, upward).wait_recv()
-                    add(p, zz, [(got[p], away)], None)
-
-            @pl.when(jnp.logical_not(has_more))
-            def _():
-                add(p, zz, [], None)
+            if away < depth - 1:
+                pl.when(has_more)(lambda: along(p, zz, away + 1, upward).wait_recv())
+            for from_y, here in kinds:
+
+                @pl.when(jnp.logical_and(inside, here))
+                def _():
+                    if from_y:
+                        over(p, zz).wait_recv()
+
+                    @pl.when(has_more)
+                    def _():
+                        add(p, zz, [(got[p], away)] if away < depth - 1 else [], None, from_y)
+
+                    @pl.when(jnp.logical_not(has_more))
+                    def _():
+                        add(p, zz, [], None, from_y)
 
             along(p, zz, away, upward).start()
 
+    done = min(4, strips)
+    late(0, done)
     for away in range(depth - 1, 0, -1):
         for p in range(2):
             pass_on(p, away, True)
             pass_on(p, away, False)
+            if away == depth - 1 and p == 1:
+                cross().wait_recv()
+                add_cross()
+                over(1, z, cross_got).start()
+            if done < strips:
+                upto = min(done + 2, strips)
+                late(done, upto)
+                done = upto
+    if done < strips:
+        late(done, strips)
 
     taps_got[pl.ds(me, 1)] = taps[...][None]
     for away in range(1, n):
@@ -333,25 +437,32 @@
         pl.when(at_high)(lambda: add(p, z, [(up_got[p], 0)], total[p]))
         pl.when(both)(lambda: add(p, z, [(up_got[p], 0), (down_got[p], 0)], total[p]))
 
+    cross().wait_send()
+    over(0, z).wait_send()
+    over(1, z, cross_got).wait_send()
     for p in range(2):
-        over(p, z).wait_send()
         for away in range(depth - 1, 0, -1):
+            up_too, down_too = over_y(p, away, True), over_y(p, away, False)
 
             @pl.when(z + away < depth)
             def _():
-                over(p, z + away).wait_send()
+                pl.when(jnp.logical_and(z + away < depth, up_too))(
+                    lambda: over(p, z + away).wait_send()
+                )
                 along(p, z + away, away, True).wait_send()
 
             @pl.when(z - away >= 0)
             def _():
-                over(p, z - away).wait_send()
+                pl.when(jnp.logical_and(z - away >= 0, down_too))(
+                    lambda: over(p, z - away).wait_send()
+                )
                 along(p, z - away, away, False).wait_send()
 
     for away in range(1, n):
         taps_copy(away).wait_send()
 
 
-def scatter_rows(gate_terms, value_terms, tap_terms):
+def scatter_rows(gate_terms, value_terms, tap_terms, rows_late, gate_full, value_full, conv_taps):
     n = lax.axis_size("fs")
     depth = n // 2
     rows, columns = gate_terms.shape[0] // n, gate_terms.shape[1]
@@ -361,13 +472,20 @@
     row_block = lambda count: pltpu.VMEM((count, rows, columns), gate_terms.dtype)
     return pl.pallas_call(
         functools.partial(scatter_kernel, n),
-        out_shape=(total, total, jax.ShapeDtypeStruct(tap_terms.shape, jnp.float32)),
-        in_specs=[vmem] * 3,
-        out_specs=(vmem,) * 3,
+        out_shape=(
+            total,
+            total,
+            jax.ShapeDtypeStruct(tap_terms.shape, jnp.float32),
+            jax.ShapeDtypeStruct((rows_late.shape[0], columns), jnp.bfloat16),
+        ),
+        in_specs=[vmem] * 4 + [pl.BlockSpec(memory_space=pl.ANY)] * 2 + [vmem],
+        out_specs=(vmem,) * 4,
         scratch_shapes=[row_block(depth)] * 2
         + [row_block(depth - 1)] * 4
         + [
             pltpu.VMEM((n,) + tap_terms.shape, jnp.float32),
+            pltpu.VMEM((rows, columns), gate_terms.dtype),
+            pltpu.VMEM((2, gate_full.shape[0], 256), gate_full.dtype),
             sems((2, depth)),
             sems((2, depth)),
             sems((2, depth)),
@@ -375,12 +493,15 @@
             sems((2, depth)),
             sems((n,)),
             sems((n,)),
+            sems,
+            sems,
+            sems((2, 2)),
         ],
         compiler_params=pltpu.CompilerParams(
             collective_id=1, has_side_effects=True, vmem_limit_bytes=60 * 1024 * 1024
         ),
         name="scatter_rows",
-    )(gate_terms, value_terms, tap_terms)
+    )(gate_terms, value_terms, tap_terms, rows_late, gate_full, value_full, conv_taps)
 
 
 def shards(x_late, x_early, w_gate, w_value, conv_taps, grad_hidden, sum_gate, sum_value, sum_taps):
@@ -388,19 +509,6 @@
     factor = 1.0 / math.sqrt(x_late.shape[0] * lax.axis_size("fs") * lax.axis_size("tp"))
     gate_full, value_full = gather_rows(w_gate, w_value)
     block_rows = lax.all_gather(x_late, "tp", axis=0, tiled=True)
-    gate_part = jnp.dot(block_rows, gate_full, preferred_element_type=jnp.float32).astype(
-        jnp.bfloat16
-    )
-    value_part = jnp.dot(block_rows, value_full, preferred_element_type=jnp.float32).astype(
-        jnp.bfloat16
-    )
-    projected = jnp.concatenate([gate_part, value_part], axis=1)
-    gate_rows = projected[:, :columns]
-    value_rows = projected[:, columns:]
-    mixed_pre, padded = causal_mix(gate_rows, conv_taps)
-    hidden = (jax.nn.gelu(mixed_pre, approximate=False) * value_rows.astype(jnp.float32)).astype(
-        jnp.bfloat16
-    )
     gathered = lax.all_gather(x_early, "tp", axis=0, tiled=True)
     gate_rows = jnp.dot(gathered, gate_full, preferred_element_type=jnp.float32).astype(
         jnp.bfloat16
@@ -428,10 +536,14 @@
     gate_terms = lax.dot_general(gathered, d_gate, outer, preferred_element_type=jnp.float32)
     value_terms = lax.dot_general(gathered, d_value, outer, preferred_element_type=jnp.float32)
     taps_padded = jnp.pad(factor * tap_terms, ((0, -tap_terms.shape[0] % 8), (0, 0)))
-    gate_total, value_total, tap_total = scatter_rows(
+    gate_total, value_total, tap_total, hidden = scatter_rows(
         (factor * gate_terms).astype(jnp.bfloat16),
         (factor * value_terms).astype(jnp.bfloat16),
         taps_padded,
+        block_rows,
+        gate_full,
+        value_full,
+        conv_taps,
     )
     tap_total = tap_total[: tap_terms.shape[0]]
     return (

time: 379 us -> 340 us (0.90)
  matrix products: 74.3 us -> 45.5 us
  Pallas kernels: 269 us -> 256 us
    dot_general x2 -> x0, matrix products: 28.9 us -> none  [the longest x1 19.9 us: shards(): jnp.dot(block_rows, value_full, preferred_element_type=jnp.float32)]
    pallas_call x1, Pallas kernels: 137 us -> 123 us  [scatter_rows(): pl.pallas_call(functools.partial(scatter_kernel, n), out_shape=(total, to...]
  transfers between devices with their start and end apart: 3 -> 3, of which waited for: 0 -> 0; matrix products, arithmetic and copies ran while one was open for 25% -> 20% of each run, Pallas kernels for 71% -> 75%
where the time goes in v2:
time: 340 us; the launch traced here: 339 us
  Pallas kernels  256 us (75%)
  matrix products  45.5 us (13%)
  other arithmetic  19.9 us (6%)
  between operations  13.9 us (4%)
    pallas_call x1, Pallas kernels, gather_rows(): pl.pallas_call(functools.partial(gather_kernel, n), out_shape=(whole, who...  132 us
    pallas_call x1, Pallas kernels, scatter_rows(): pl.pallas_call(functools.partial(scatter_kernel, n), out_shape=(total, to...  123 us
    convert_element_type x1, other arithmetic, shards(): (upstream * jax.nn.gelu(mixed_pre, approximate=False)).astype(jnp.bfloat16)  10.9 us
    dot_general x1, matrix products, shards(): lax.dot_general(gathered, d_gate, outer, preferred_element_type=jnp.float32)  9.11 us
    dot_general x1, matrix products, shards(): jnp.dot(gathered, gate_full, preferred_element_type=jnp.float32)  8.55 us
    dot_general x1, matrix products, shards(): jnp.dot(gathered, value_full, preferred_element_type=jnp.float32)  7.5 us
    dot_general x1, matrix products, shards(): lax.dot_general(gathered, d_value, outer, preferred_element_type=jnp.floa...  6.97 us
  transfers between devices with their start and end apart: 3, of which 0 were waited for; matrix products, arithmetic and copies ran while one was open for 20% of the time, Pallas kernels for 75%

profile of v2, /device:TPU:0, one launch (start us, length us, event | category | flops | bytes accessed | tf_op | source)
XLA Modules:
  0.0 339.5 jit_solution(18091684998954457279)
XLA Ops:
  7.2 0.0 all-gather.3.cloned.1.call-start
  7.2 0.7 all-gather.3.cloned.1.call-update
  7.9 0.0 all-gather.5.cloned.1.call-start
  7.9 0.7 all-gather.5.cloned.1.call-update
  8.6 0.0 reduce-scatter.2.cloned.1.call-start
  8.7 0.9 slice_reduce_fusion.2
  9.6 132.3 %gather_rows.1 = (bf16[2048,1408]{1,0:T(8,128)(2,1)}, bf16[2048,1408]{1,0:T(8,128)(2,1)}) custom-call(bf16[256,1408]{1,0:T(8,128)(2,1)} %refs_0_.1, bf16[256,1408]{1,0:T(8,128)(2,1)} %refs_1_.1), custom_call_target="tpu_custom_call" | custom-call | tf_op jit(solution)/shard_map/gather_rows/pallas_call | solution.py:189
  141.9 0.0 all-gather.3.cloned.1.call-done
  142.0 8.6 %convert_bitcast_fusion = f32[768,1408]{1,0:T(8,128)S(1)} fusion(bf16[768,2048]{1,0:T(8,128)(2,1)} %all-gather.3.cloned.1.call-done, bf16[2048,1408]{1,0:T(8,128)(2,1)} %get-tuple-element.12.refs_4_), kind=kOutput, calls=%fused_computation.17 | convolution fusion | flops 4431347712 | bytes 13238272 | tf_op jit(solution)/shard_map/dot_general | solution.py:513
  150.6 10.9 %fusion.3 = (bf16[768,1408]{1,0:T(8,128)(2,1)S(1)}, f32[768,1408]{1,0:T(8,128)S(1)}) fusion(bf16[768,1408]{1,0:T(8,128)(2,1)S(1)} %copy-done.2, f32[768,1408]{1,0:T(8,128)S(1)} %convert_bitcast_fusion, f32[1408]{0:T(1024)S(1)} %get-tuple-element.22, f32[1408]{0:T(1024)S(1)} %get-tuple-element.21, f32[1408]{0:T(1024)S(1)} %get-tuple-element.20), kind=kLoop, calls=%fused_computation.10 | loop fusion | flops 77856768 | bytes 12993024 | tf_op jit(solution)/shard_map/convert_element_type | solution.py:524
  161.5 7.5 %fusion.2 = f32[768,1408]{1,0:T(8,128)S(1)} fusion(bf16[768,1408]{1,0:T(8,128)(2,1)S(1)} %copy-done.2, f32[768,1408]{1,0:T(8,128)S(1)} %get-tuple-element.24, bf16[768,2048]{1,0:T(8,128)(2,1)} %all-gather.3.cloned.1.call-done, bf16[2048,1408]{1,0:T(8,128)(2,1)S(1)} %copy-done), kind=kOutput, calls=%fused_computation.9 | convolution fusion | flops 4443242496 | bytes 19726336 | tf_op jit(solution)/shard_map/dot_general | solution.py:516
  169.0 3.9 %multiply_reduce_fusion.2 = (f32[1408]{0:T(1024)S(1)}, f32[1408]{0:T(1024)S(1)}, f32[1408]{0:T(1024)S(1)}, bf16[768,1408]{1,0:T(8,128)(2,1)}) fusion(f32[768,1408]{1,0:T(8,128)S(1)} %fusion.2, f32[768,1408]{1,0:T(8,128)S(1)} %convert_bitcast_fusion, f32[1408]{0:T(1024)S(1)} %get-tuple-element.22, f32[1408]{0:T(1024)S(1)} %get-tuple-element.21, ...), kind=kLoop, calls=%fused_computation.20 | loop fusion | flops 12971904 | bytes 10847232 | tf_op jit(solution)/shard_map/reduce_sum | solution.py:40
  172.9 6.7 %fusion.17 = f32[768,2048]{1,0:T(8,128)S(1)} fusion(bf16[768,1408]{1,0:T(8,128)(2,1)} %get-tuple-element.25, bf16[2048,1408]{1,0:T(8,128)(2,1)S(1)} %bitcast.21), kind=kOutput, calls=%fused_computation.47 | convolution fusion | flops 4429185024 | bytes 14221312 | tf_op jit(solution)/shard_map/dot_general | solution.py:528
  179.6 6.7 %add_convert_fusion = bf16[768,2048]{1,0:T(8,128)(2,1)} fusion(f32[768,2048]{1,0:T(8,128)S(1)} %fusion.17, bf16[768,1408]{1,0:T(8,128)(2,1)S(1)} %get-tuple-element.23, bf16[2048,1408]{1,0:T(8,128)(2,1)S(1)} %copy-done), kind=kOutput, calls=%fused_computation.6 | convolution fusion | flops 4432330752 | bytes 17367040 | tf_op jit(solution)/shard_map/dot_general | solution.py:529
  186.3 0.0 reduce-scatter.2.cloned.1.call-update
  186.4 0.6 pad.14.refs_2_
  187.0 9.1 %fusion.refs_0_ = bf16[2048,1408]{1,0:T(8,128)(2,1)} fusion(bf16[768,1408]{1,0:T(8,128)(2,1)} %get-tuple-element.25, bf16[768,2048]{1,0:T(8,128)(2,1)} %all-gather.3.cloned.1.call-done), kind=kOutput, calls=%fused_computation.2 | convolution fusion | flops 4434952192 | bytes 11075584 | tf_op jit(solution)/shard_map/dot_general | solution.py:536
  196.1 7.0 %fusion.1.refs_1_ = bf16[2048,1408]{1,0:T(8,128)(2,1)} fusion(bf16[768,1408]{1,0:T(8,128)(2,1)S(1)} %get-tuple-element.23, bf16[768,2048]{1,0:T(8,128)(2,1)S(1)} %copy-done.7), kind=kOutput, calls=%fused_computation.3 | convolution fusion | flops 4434952192 | bytes 11075584 | tf_op jit(solution)/shard_map/dot_general | solution.py:537
  203.1 123.4 %scatter_rows.1 = (f32[256,1408]{1,0:T(8,128)}, f32[256,1408]{1,0:T(8,128)}, f32[8,1408]{1,0:T(8,128)}, bf16[768,1408]{1,0:T(8,128)(2,1)}) custom-call(bf16[2048,1408]{1,0:T(8,128)(2,1)} %fusion.refs_0_, bf16[2048,1408]{1,0:T(8,128)(2,1)} %fusion.1.refs_1_, f32[8,1408]{1,0:T(8,128)} %pad.14.refs_2_, bf16[768,2048]{1,0:T(8,128)(2,1)} %all-gather.5.cloned.1.call-done.refs_3_, ...), custom_call_target="tpu_custom_call" | custom-call | tf_op jit(solution)/shard_map/scatter_rows/pallas_call | solution.py:473
  326.5 0.0 copy-start.3
  326.6 3.2 add.45
  329.7 1.2 add.46
  331.0 0.6 slice_add_fusion
  331.6 1.3 copy.19
  (26 shorter events, 0.1 us)
Async XLA Ops:
  7.2 134.8 %all-gather.3.cloned.1.call-start = ((), (), s32[]{:S(2)}) async-start(), calls=%async_computation.1 | async-start | bytes 3932160 | tf_op jit(solution)/shard_map/all_gather | solution.py:512
  7.9 195.2 %all-gather.5.cloned.1.call-start = ((), (), s32[]{:S(2)}) async-start(), calls=%async_computation.2 | async-start | bytes 3932160 | tf_op jit(solution)/shard_map/all_gather | solution.py:511
  8.6 323.0 %reduce-scatter.2.cloned.1.call-start = ((), (), s32[]{:S(2)}) async-start(), calls=%async_computation.3 | async-start | bytes 3932160 | tf_op jit(solution)/shard_map/reduce_scatter | solution.py:526
  141.9 8.6 %copy-start.2 = (bf16[768,1408]{1,0:T(8,128)(2,1)S(1)}, bf16[768,1408]{1,0:T(8,128)(2,1)}, u32[]{:S(2)}) copy-start(bf16[768,1408]{1,0:T(8,128)(2,1)} %param.14) | copy-start | bytes 6488068
  150.5 10.9 %copy-start = (bf16[2048,1408]{1,0:T(8,128)(2,1)S(1)}, bf16[2048,1408]{1,0:T(8,128)(2,1)}, u32[]{:S(2)}) copy-start(bf16[2048,1408]{1,0:T(8,128)(2,1)} %get-tuple-element.11.refs_5_) | copy-start | bytes 17301508
  150.5 22.4 %slice-start = ((s8[5767168]{0:T(1024)(128)(4,1)}), s8[4194304]{0:T(1024)(128)(4,1)S(1)}, s32[]{:S(2)}) async-start(s8[5767168]{0:T(1024)(128)(4,1)} %bitcast.20), calls=%async_computation.4 | async-start | bytes 8388608
  161.5 11.5 %slice-start.1 = ((s8[5767168]{0:T(1024)(128)(4,1)}), s8[1572864]{0:T(1024)(128)(4,1)S(1)}, s32[]{:S(2)}) async-start(s8[5767168]{0:T(1024)(128)(4,1)} %bitcast.20), calls=%async_computation.5 | async-start | bytes 3145728
  187.0 9.1 %copy-start.7 = (bf16[768,2048]{1,0:T(8,128)(2,1)S(1)}, bf16[768,2048]{1,0:T(8,128)(2,1)}, u32[]{:S(2)}) copy-start(bf16[768,2048]{1,0:T(8,128)(2,1)} %all-gather.3.cloned.1.call-done) | copy-start | bytes 9437188
  326.5 3.2 copy-start.3
  326.5 3.2 copy-start.4
  326.5 4.5 %copy-start.5 = (f32[3,1408]{1,0:T(4,128)S(1)}, f32[3,1408]{1,0:T(4,128)}, u32[]{:S(2)}) copy-start(f32[3,1408]{1,0:T(4,128)} %param.17) | copy-start | bytes 50692
  326.5 4.5 %copy-start.6 = (f32[8,1408]{1,0:T(8,128)S(1)}, f32[8,1408]{1,0:T(8,128)}, u32[]{:S(2)}) copy-start(f32[8,1408]{1,0:T(8,128)} %get-tuple-element.16) | copy-start | bytes 135172
  326.5 5.1 %copy-start.1 = (bf16[768,1408]{1,0:T(8,128)(2,1)S(1)}, bf16[768,1408]{1,0:T(8,128)(2,1)}, u32[]{:S(2)}) copy-start(bf16[768,1408]{1,0:T(8,128)(2,1)} %get-tuple-element.31) | copy-start | bytes 6488068
Sparse Core Ops, SparseCore 0:
  9.5 31.2 all-gather.2
  42.4 28.4 all-gather.4
  186.4 36.8 reduce-scatter.1

commit v3 on v2

--- a/solution.py
+++ b/solution.py
@@ -207,13 +207,14 @@
     )(w_gate, w_value)
 
 
-def scatter_kernel(n, *refs):
-    terms, taps, rows_late, weights, conv = refs[:2], refs[2], refs[3], refs[4:6], refs[6]
-    total, taps_total, hidden = refs[7:9], refs[9], refs[10]
-    y_got, up_got, down_got, taps_got = refs[11:13], refs[13:15], refs[15:17], refs[17]
-    cross_got, strip = refs[18], refs[19]
-    y_out, y_in, z_out, up_in, down_in, taps_out, taps_in = refs[20:27]
-    cross_out, cross_in, strip_in = refs[27:]
+def scatter_kernel(n, factor, *refs):
+    flipped, deltas, taps, rows_late = refs[0], refs[1:3], refs[3], refs[4]
+    weights, conv = refs[5:7], refs[7]
+    total, taps_total, hidden = refs[8:10], refs[10], refs[11]
+    y_got, up_got, down_got, taps_got = refs[12:14], refs[14:16], refs[16:18], refs[18]
+    cross_got, strip, terms = refs[19], refs[20], refs[21:23]
+    y_out, y_in, z_out, up_in, down_in, taps_out, taps_in = refs[23:30]
+    cross_out, cross_in, strip_in = refs[30:]
     rows = total[0].shape[0]
     depth = n // 2
     step = math.gcd(rows, 32)
@@ -269,6 +270,11 @@
     def start_of(zz, yy):
         return pl.multiple_of((zz * 2 + yy) * rows, rows)
 
+    def make(p, zz, yy):
+        at = pl.ds(start_of(zz, yy), rows)
+        term = jnp.dot(flipped[at, :], deltas[p][...], preferred_element_type=jnp.float32)
+        terms[p][at, :] = (factor * term).astype(terms[p].dtype)
+
     def over(p, zz, source=None):
         return pltpu.make_async_remote_copy(
             src_ref=terms[p].at[pl.ds(start_of(zz, 1 - y), rows)] if source is None else source,
@@ -350,16 +356,28 @@
     for copy in fetch(0):
         copy.start()
     greet(n, me)
+    make(1, mate, 1 - y)
     cross().start()
-    for away in range(depth - 1, 0, -1):
+
+    def send_terms(i, _):
+        away = depth - 1 - i
         for p in range(2):
-            up_too, down_too = over_y(p, away, True), over_y(p, away, False)
-            pl.when(jnp.logical_and(z + away < depth, up_too))(
-                lambda: over(p, z + away).start()
-            )
-            pl.when(jnp.logical_and(z - away >= 0, down_too))(
-                lambda: over(p, z - away).start()
-            )
+            up_too = z + away < depth
+            down_too = z - away >= 0
+            if p == 1:
+                up_too = jnp.logical_and(up_too, jnp.logical_or(away > 1, odd))
+                down_too = jnp.logical_and(down_too, jnp.logical_or(away > 1, even))
+            for here, zz in ((up_too, z + away), (down_too, z - away)):
+
+                @pl.when(here)
+                def _():
+                    make(p, zz, 1 - y)
+                    over(p, zz).start()
+
+        return 0
+
+    lax.fori_loop(0, depth - 1, send_terms, 0)
+    make(0, z, 1 - y)
     over(0, z).start()
     for away in range(1, n):
         taps_copy(away).start()
@@ -394,7 +412,15 @@
 
             along(p, zz, away, upward).start()
 
-    done = min(4, strips)
+    make(1, z, 1 - y)
+
+    def own_terms(zz, _):
+        for p in range(2):
+            make(p, zz, y)
+        return 0
+
+    lax.fori_loop(0, depth, own_terms, 0)
+    done = min(1, strips)
     late(0, done)
     for away in range(depth - 1, 0, -1):
         for p in range(2):
@@ -462,30 +488,32 @@
         taps_copy(away).wait_send()
 
 
-def scatter_rows(gate_terms, value_terms, tap_terms, rows_late, gate_full, value_full, conv_taps):
+def scatter_rows(factor, flipped, d_gate, d_value, tap_terms, rows_late, gate_full, value_full, conv_taps):
     n = lax.axis_size("fs")
     depth = n // 2
-    rows, columns = gate_terms.shape[0] // n, gate_terms.shape[1]
+    rows, columns = flipped.shape[0] // n, d_gate.shape[1]
     sems = pltpu.SemaphoreType.DMA
     vmem = pl.BlockSpec(memory_space=pltpu.VMEM)
     total = jax.ShapeDtypeStruct((rows, columns), jnp.float32)
-    row_block = lambda count: pltpu.VMEM((count, rows, columns), gate_terms.dtype)
+    row_block = lambda count: pltpu.VMEM((count, rows, columns), d_gate.dtype)
     return pl.pallas_call(
-        functools.partial(scatter_kernel, n),
+        functools.partial(scatter_kernel, n, factor),
         out_shape=(
             total,
             total,
             jax.ShapeDtypeStruct(tap_terms.shape, jnp.float32),
             jax.ShapeDtypeStruct((rows_late.shape[0], columns), jnp.bfloat16),
         ),
-        in_specs=[vmem] * 4 + [pl.BlockSpec(memory_space=pl.ANY)] * 2 + [vmem],
+        in_specs=[vmem] * 5 + [pl.BlockSpec(memory_space=pl.ANY)] * 2 + [vmem],
         out_specs=(vmem,) * 4,
         scratch_shapes=[row_block(depth)] * 2
         + [row_block(depth - 1)] * 4
         + [
             pltpu.VMEM((n,) + tap_terms.shape, jnp.float32),
-            pltpu.VMEM((rows, columns), gate_terms.dtype),
+            pltpu.VMEM((rows, columns), d_gate.dtype),
             pltpu.VMEM((2, gate_full.shape[0], 256), gate_full.dtype),
+            pltpu.VMEM((n * rows, columns), d_gate.dtype),
+            pltpu.VMEM((n * rows, columns), d_gate.dtype),
             sems((2, depth)),
             sems((2, depth)),
             sems((2, depth)),
@@ -501,7 +529,7 @@
             collective_id=1, has_side_effects=True, vmem_limit_bytes=60 * 1024 * 1024
         ),
         name="scatter_rows",
-    )(gate_terms, value_terms, tap_terms, rows_late, gate_full, value_full, conv_taps)
+    )(flipped, d_gate, d_value, tap_terms, rows_late, gate_full, value_full, conv_taps)
 
 
 def shards(x_late, x_early, w_gate, w_value, conv_taps, grad_hidden, sum_gate, sum_value, sum_taps):
@@ -532,13 +560,12 @@
         scatter_dimension=0,
         tiled=True,
     )
-    outer = (((0,), (0,)), ((), ()))
-    gate_terms = lax.dot_general(gathered, d_gate, outer, preferred_element_type=jnp.float32)
-    value_terms = lax.dot_general(gathered, d_value, outer, preferred_element_type=jnp.float32)
     taps_padded = jnp.pad(factor * tap_terms, ((0, -tap_terms.shape[0] % 8), (0, 0)))
     gate_total, value_total, tap_total, hidden = scatter_rows(
-        (factor * gate_terms).astype(jnp.bfloat16),
-        (factor * value_terms).astype(jnp.bfloat16),
+        factor,
+        gathered.T,
+        d_gate,
+        d_value,
         taps_padded,
         block_rows,
         gate_full,

time: 340 us -> 324 us (0.953)
  matrix products: 45.5 us -> 26.3 us
  local copies, waits for them, and re-layouts: 2.93 us -> 6.95 us
    dot_general x2 -> x0, matrix products: 16.1 us -> none  [the longest x1 9.11 us: shards(): lax.dot_general(gathered, d_gate, outer, preferred_element_type=jnp.float32)]
  transfers between devices with their start and end apart: 3 -> 3, of which waited for: 0 -> 0; matrix products, arithmetic and copies ran while one was open for 20% -> 15% of each run, Pallas kernels for 75% -> 79%
where the time goes in v3:
time: 324 us; the launch traced here: 323 us
  Pallas kernels  255 us (79%)
  matrix products  26.3 us (8%)
  other arithmetic  19.1 us (6%)
  between operations  14 us (4%)
  local copies, waits for them, and re-layouts  6.95 us (2%)
    pallas_call x1, Pallas kernels, gather_rows(): pl.pallas_call(functools.partial(gather_kernel, n), out_shape=(whole, who...  132 us
    pallas_call x1, Pallas kernels, scatter_rows(): pl.pallas_call(functools.partial(scatter_kernel, n, factor), out_shape=(t...  123 us
    convert_element_type x1, other arithmetic, shards(): (upstream * jax.nn.gelu(mixed_pre, approximate=False)).astype(jnp.bfloat16)  10.9 us
    dot_general x1, matrix products, shards(): jnp.dot(gathered, gate_full, preferred_element_type=jnp.float32)  8.55 us
    dot_general x1, matrix products, shards(): lax.dot_general(d_value, value_full, contract, preferred_element_type=jnp...  6.6 us
  transfers between devices with their start and end apart: 3, of which 0 were waited for; matrix products, arithmetic and copies ran while one was open for 15% of the time, Pallas kernels for 79%

profile of v3, /device:TPU:0, one launch (start us, length us, event | category | flops | bytes accessed | tf_op | source)
XLA Modules:
  0.0 323.2 jit_solution(6098155083773097308)
XLA Ops:
  7.2 0.0 all-gather.3.cloned.1.call-start
  7.2 0.7 all-gather.3.cloned.1.call-update
  7.9 0.0 all-gather.5.cloned.1.call-start
  7.9 0.7 all-gather.5.cloned.1.call-update
  8.6 0.0 reduce-scatter.2.cloned.1.call-start
  8.7 0.9 slice_reduce_fusion.2
  9.6 132.3 %gather_rows.1 = (bf16[2048,1408]{1,0:T(8,128)(2,1)}, bf16[2048,1408]{1,0:T(8,128)(2,1)}) custom-call(bf16[256,1408]{1,0:T(8,128)(2,1)} %refs_0_.1, bf16[256,1408]{1,0:T(8,128)(2,1)} %refs_1_.1), custom_call_target="tpu_custom_call" | custom-call | tf_op jit(solution)/shard_map/gather_rows/pallas_call | solution.py:189
  141.9 0.0 all-gather.3.cloned.1.call-done
  141.9 0.0 copy-start.6
  142.0 8.6 %convert_bitcast_fusion = f32[768,1408]{1,0:T(8,128)S(1)} fusion(bf16[768,2048]{1,0:T(8,128)(2,1)} %all-gather.3.cloned.1.call-done, bf16[2048,1408]{1,0:T(8,128)(2,1)} %get-tuple-element.12.refs_5_), kind=kOutput, calls=%fused_computation.13 | convolution fusion | flops 4431347712 | bytes 13238272 | tf_op jit(solution)/shard_map/dot_general | solution.py:541
  150.6 10.9 %fusion.1 = (bf16[768,1408]{1,0:T(8,128)(2,1)S(1)}, f32[768,1408]{1,0:T(8,128)S(1)}) fusion(bf16[768,1408]{1,0:T(8,128)(2,1)S(1)} %copy-done.6, f32[768,1408]{1,0:T(8,128)S(1)} %convert_bitcast_fusion, f32[1408]{0:T(1024)S(1)} %get-tuple-element.22, f32[1408]{0:T(1024)S(1)} %get-tuple-element.21, f32[1408]{0:T(1024)S(1)} %get-tuple-element.20), kind=kLoop, calls=%fused_computation.6 | loop fusion | flops 77856768 | bytes 12993024 | tf_op jit(solution)/shard_map/convert_element_type | solution.py:552
  161.5 6.1 %fusion = f32[768,1408]{1,0:T(8,128)S(1)} fusion(bf16[768,1408]{1,0:T(8,128)(2,1)S(1)} %copy-done.6, f32[768,1408]{1,0:T(8,128)S(1)} %get-tuple-element.24, bf16[768,2048]{1,0:T(8,128)(2,1)S(1)} %copy-done.3, bf16[2048,1408]{1,0:T(8,128)(2,1)S(1)} %copy-done.2), kind=kOutput, calls=%fused_computation.5 | convolution fusion | flops 4443242496 | bytes 19726336 | tf_op jit(solution)/shard_map/dot_general | solution.py:544
  167.6 3.2 multiply_reduce_fusion.2
  170.8 5.1 %fusion.15 = f32[768,2048]{1,0:T(8,128)S(1)} fusion(bf16[768,1408]{1,0:T(8,128)(2,1)S(1)} %get-tuple-element.25.refs_1_, bf16[2048,1408]{1,0:T(8,128)(2,1)S(1)} %bitcast.15), kind=kOutput, calls=%fused_computation.43 | convolution fusion | flops 4429185024 | bytes 14221312 | tf_op jit(solution)/shard_map/dot_general | solution.py:556
  175.9 6.6 %add_convert_fusion = bf16[768,2048]{1,0:T(8,128)(2,1)} fusion(f32[768,2048]{1,0:T(8,128)S(1)} %fusion.15, bf16[768,1408]{1,0:T(8,128)(2,1)S(1)} %get-tuple-element.23.refs_2_, bf16[2048,1408]{1,0:T(8,128)(2,1)S(1)} %copy-done.2), kind=kOutput, calls=%fused_computation.2 | convolution fusion | flops 4432330752 | bytes 17367040 | tf_op jit(solution)/shard_map/dot_general | solution.py:557
  182.5 0.0 reduce-scatter.2.cloned.1.call-update
  182.6 0.6 pad.14.refs_3_
  183.2 1.2 copy-done.4
  184.4 2.8 copy.15
  187.2 123.0 %scatter_rows.1 = (f32[256,1408]{1,0:T(8,128)}, f32[256,1408]{1,0:T(8,128)}, f32[8,1408]{1,0:T(8,128)}, bf16[768,1408]{1,0:T(8,128)(2,1)}) custom-call(bf16[2048,768]{1,0:T(8,128)(2,1)} %bitcast.13, bf16[768,1408]{1,0:T(8,128)(2,1)} %copy-done.1, bf16[768,1408]{1,0:T(8,128)(2,1)} %copy-done, f32[8,1408]{1,0:T(8,128)} %pad.14.refs_3_, ...), custom_call_target="tpu_custom_call" | custom-call | tf_op jit(solution)/shard_map/scatter_rows/pallas_call | solution.py:499
  310.3 3.2 add.45
  313.5 1.2 add.46
  314.7 0.6 slice_add_fusion
  315.4 1.3 copy.17
  (31 shorter events, 0.1 us)
Async XLA Ops:
  7.2 134.8 %all-gather.3.cloned.1.call-start = ((), (), s32[]{:S(2)}) async-start(), calls=%async_computation.1 | async-start | bytes 3932160 | tf_op jit(solution)/shard_map/all_gather | solution.py:540
  7.9 179.3 %all-gather.5.cloned.1.call-start = ((), (), s32[]{:S(2)}) async-start(), calls=%async_computation.2 | async-start | bytes 3932160 | tf_op jit(solution)/shard_map/all_gather | solution.py:539
  8.6 306.7 %reduce-scatter.2.cloned.1.call-start = ((), (), s32[]{:S(2)}) async-start(), calls=%async_computation.3 | async-start | bytes 3932160 | tf_op jit(solution)/shard_map/reduce_scatter | solution.py:554
  141.9 8.6 %copy-start.6 = (bf16[768,1408]{1,0:T(8,128)(2,1)S(1)}, bf16[768,1408]{1,0:T(8,128)(2,1)}, u32[]{:S(2)}) copy-start(bf16[768,1408]{1,0:T(8,128)(2,1)} %param.14) | copy-start | bytes 6488068
  142.0 19.5 %copy-start.3 = (bf16[768,2048]{1,0:T(8,128)(2,1)S(1)}, bf16[768,2048]{1,0:T(8,128)(2,1)}, u32[]{:S(2)}) copy-start(bf16[768,2048]{1,0:T(8,128)(2,1)} %all-gather.3.cloned.1.call-done) | copy-start | bytes 9437188
  150.5 10.9 %copy-start.2 = (bf16[2048,1408]{1,0:T(8,128)(2,1)S(1)}, bf16[2048,1408]{1,0:T(8,128)(2,1)}, u32[]{:S(2)}) copy-start(bf16[2048,1408]{1,0:T(8,128)(2,1)} %get-tuple-element.11.refs_6_) | copy-start | bytes 17301508
  150.5 20.2 %slice-start = ((s8[5767168]{0:T(1024)(128)(4,1)}), s8[4194304]{0:T(1024)(128)(4,1)S(1)}, s32[]{:S(2)}) async-start(s8[5767168]{0:T(1024)(128)(4,1)} %bitcast.14), calls=%async_computation.4 | async-start | bytes 8388608
  161.5 14.4 %copy-start = (bf16[768,1408]{1,0:T(8,128)(2,1)}, bf16[768,1408]{1,0:T(8,128)(2,1)S(1)}, u32[]{:S(2)}) copy-start(bf16[768,1408]{1,0:T(8,128)(2,1)S(1)} %get-tuple-element.23.refs_2_) | copy-start | bytes 6488068
  161.5 9.3 %slice-start.1 = ((s8[5767168]{0:T(1024)(128)(4,1)}), s8[1572864]{0:T(1024)(128)(4,1)S(1)}, s32[]{:S(2)}) async-start(s8[5767168]{0:T(1024)(128)(4,1)} %bitcast.14), calls=%async_computation.5 | async-start | bytes 3145728
  170.8 5.1 %copy-start.1 = (bf16[768,1408]{1,0:T(8,128)(2,1)}, bf16[768,1408]{1,0:T(8,128)(2,1)S(1)}, u32[]{:S(2)}) copy-start(bf16[768,1408]{1,0:T(8,128)(2,1)S(1)} %get-tuple-element.25.refs_1_) | copy-start | bytes 6488068
  182.5 1.9 copy-start.4
  310.2 3.2 %copy-start.7 = (f32[256,1408]{1,0:T(8,128)S(1)}, f32[256,1408]{1,0:T(8,128)}, u32[]{:S(2)}) copy-start(f32[256,1408]{1,0:T(8,128)} %param.16) | copy-start | bytes 4325380
  310.2 3.2 %copy-start.8 = (f32[256,1408]{1,0:T(8,128)S(1)}, f32[256,1408]{1,0:T(8,128)}, u32[]{:S(2)}) copy-start(f32[256,1408]{1,0:T(8,128)} %get-tuple-element.15) | copy-start | bytes 4325380
  310.3 4.5 %copy-start.9 = (f32[3,1408]{1,0:T(4,128)S(1)}, f32[3,1408]{1,0:T(4,128)}, u32[]{:S(2)}) copy-start(f32[3,1408]{1,0:T(4,128)} %param.17) | copy-start | bytes 50692
  310.3 4.5 %copy-start.10 = (f32[8,1408]{1,0:T(8,128)S(1)}, f32[8,1408]{1,0:T(8,128)}, u32[]{:S(2)}) copy-start(f32[8,1408]{1,0:T(8,128)} %get-tuple-element.16) | copy-start | bytes 135172
  310.3 5.1 %copy-start.5 = (bf16[768,1408]{1,0:T(8,128)(2,1)S(1)}, bf16[768,1408]{1,0:T(8,128)(2,1)}, u32[]{:S(2)}) copy-start(bf16[768,1408]{1,0:T(8,128)(2,1)} %get-tuple-element.31) | copy-start | bytes 6488068
Sparse Core Ops, SparseCore 0:
  9.5 31.2 all-gather.2
  42.4 28.4 all-gather.4
  182.7 36.8 reduce-scatter.1
